TPU v7x, 32 devices: a whole 2x2x4 slice. The times are simulated.
32 devices in a mesh: sp: 8 (over z, x), tp: 4 (over y, core).
Axes of the slice: x: 2, y: 2, z: 4, core: 2. Of those that a mesh axis runs over, the one named last changes fastest.
Arguments:
- residual_in: bfloat16 [2048, 2048], P('sp', 'tp'), may hold values from -6 to 6
- conv_input: bfloat16 [2048, 512], P('sp', 'tp'), may hold values from -6 to 6
- outer_gate: bfloat16 [2048, 512], P('sp', 'tp'), may hold values from -6 to 6
- inner_gate: bfloat16 [2048, 512], P('sp', 'tp'), may hold values from -6 to 6
- documents: int32 [2048], P('sp'), may hold values from 0 to 3, as said below
- conv_taps: float32 [3, 512], P(None, 'tp'), may hold values from -3 to 3
- mixer_gain: float32 [512], replicated, may hold values from 0.1 to 1.9
- output_weight: bfloat16 [512, 2048], P(None, 'tp'), may hold values from -0.25 to 0.25
- ffn_gain: float32 [2048], P('tp'), may hold values from 0.1 to 1.9
- routes: int32 [2048, 2], P('sp'), may hold values from 0 to 7, all different within a row; in each aligned block of 256 rows (0 to 255, 256 to 511, ...) at most 128 rows name the same one
- route_weights: float32 [2048, 2], P('sp'), may hold values from 0.1 to 0.9
- expert_gate: bfloat16 [8, 2048, 3584], P('sp', None, 'tp'), may hold values from -0.125 to 0.125
- expert_up: bfloat16 [8, 2048, 3584], P('sp', None, 'tp'), may hold values from -0.125 to 0.125
- expert_down: bfloat16 [8, 3584, 2048], P('sp', 'tp'), may hold values from -0.09375 to 0.09375
Outputs:
- layer_out: bfloat16 [2048, 2048], P('sp', 'tp')
Inputs may be any that keep to these rules, and one draw needn't show every extreme that they name: Document numbers never fall along the positions, and each of the 4 documents occurs. Every document has 256 to 768 positions, and one has exactly 768. `routes`: the two experts of a position differ. Among the 256 positions of one index of sp no expert is named more than 128 times, a bound that some block reaches.
All inputs are finite; a program needn't handle non-finite values.
Results may differ from a plain program's by a relative error of at most 0.0058.
Values may be sent and summed in bfloat16 or wider, within the bound.
A program may use at most 64 MiB of HBM per device.

v0:
```python
import jax
import jax.numpy as jnp
from jax import lax
from jax.sharding import PartitionSpec as P

EPS = 1e-06


def from_behind(block, axis, distance):
    devices = range(lax.axis_size(axis))
    route = [(i - distance, i) for i in devices if i - distance in devices]
    return lax.ppermute(block, axis, route)


def slot_tables(routes, experts, capacity):
    tokens = routes.shape[0]
    flattened = routes.reshape(-1)
    onehot = (flattened[:, None] == jnp.arange(experts, dtype=jnp.int32)[None, :]).astype(jnp.int32)
    earlier = jnp.cumsum(onehot, axis=0) - onehot
    position_in = jnp.sum(earlier * onehot, axis=1)
    target = flattened * capacity + position_in
    owners = (
        jnp.full((experts * capacity,), tokens, jnp.int32)
        .at[target]
        .set(jnp.arange(2 * tokens, dtype=jnp.int32) // 2)
    )
    return (target, owners)


def per_device(
    residual_in,
    conv_input,
    outer_gate,
    inner_gate,
    documents,
    conv_taps,
    mixer_gain,
    output_weight,
    ffn_gain,
    routes,
    route_weights,
    expert_gate,
    expert_up,
    expert_down,
):
    tokens_here = residual_in.shape[0]
    local_features = residual_in.shape[1]
    conv_value = (inner_gate.astype(jnp.float32) * conv_input.astype(jnp.float32)).astype(
        jnp.bfloat16
    )
    doc_marks = documents.astype(jnp.bfloat16)
    before_rows, before_docs = from_behind((conv_value[-2:], doc_marks[-2:]), "sp", 1)
    joined_rows = jnp.concatenate([before_rows, conv_value], axis=0).astype(jnp.float32)
    joined_docs = jnp.concatenate([before_docs, doc_marks], axis=0)
    same_one = (joined_docs[1:-1] == doc_marks).astype(jnp.float32)[:, None]
    same_two = (joined_docs[:-2] == doc_marks).astype(jnp.float32)[:, None]
    conv_sum = (
        conv_taps[2] * joined_rows[2:]
        + conv_taps[1] * joined_rows[1:-1] * same_one
        + conv_taps[0] * joined_rows[:-2] * same_two
    )
    mixed = (outer_gate.astype(jnp.float32) * conv_sum).astype(jnp.bfloat16)
    piece_f = lax.all_gather(mixed, "tp", axis=1, tiled=True).astype(jnp.float32)
    scaled = (piece_f * mixer_gain).astype(jnp.bfloat16)
    accum = jnp.dot(scaled, output_weight, preferred_element_type=jnp.float32)
    squares = jnp.sum(piece_f * piece_f, axis=1)
    mix_scale = lax.rsqrt(squares / mixer_gain.shape[0] + EPS)
    hidden_state = residual_in.astype(jnp.float32) + accum * mix_scale[:, None]
    feature_total = lax.psum(jnp.sum(hidden_state * hidden_state, axis=1), "tp")
    model_width = local_features * lax.axis_size("tp")
    normed = (
        hidden_state * lax.rsqrt(feature_total / model_width + EPS)[:, None] * ffn_gain
    ).astype(jnp.bfloat16)
    experts = lax.axis_size("sp") * expert_gate.shape[0]
    capacity = 4 * tokens_here // experts
    target, owners = slot_tables(routes, experts, capacity)
    padded = jnp.concatenate([normed, jnp.zeros((1, local_features), jnp.bfloat16)], axis=0)
    outgoing = padded[owners].reshape(experts, capacity, local_features)
    slices_in = lax.all_to_all(outgoing, "sp", split_axis=0, concat_axis=0, tiled=True)
    arrived = lax.all_gather(slices_in, "tp", axis=2, tiled=True)
    expert_in = arrived.reshape(-1, model_width)
    gate = jnp.dot(expert_in, expert_gate[0], preferred_element_type=jnp.float32)
    upper = jnp.dot(expert_in, expert_up[0], preferred_element_type=jnp.float32)
    act = (jax.nn.silu(gate) * upper).astype(jnp.bfloat16)
    partial_out = jnp.dot(act, expert_down[0], preferred_element_type=jnp.float32)
    summed = lax.psum_scatter(
        partial_out.astype(jnp.bfloat16), "tp", scatter_dimension=1, tiled=True
    )
    returned = lax.all_to_all(
        summed.reshape(experts, capacity, local_features),
        "sp",
        split_axis=0,
        concat_axis=0,
        tiled=True,
    )
    picked = returned.reshape(experts * capacity, local_features)[target].astype(jnp.float32)
    picked = picked.reshape(tokens_here, 2, local_features)
    routed = jnp.sum(picked * route_weights[:, :, None], axis=1)
    return (hidden_state + routed).astype(jnp.bfloat16)


def solution(mesh):
    placed = (
        P("sp", "tp"),
        P("sp", "tp"),
        P("sp", "tp"),
        P("sp", "tp"),
        P("sp"),
        P(None, "tp"),
        P(),
        P(None, "tp"),
        P("tp"),
        P("sp", None),
        P("sp", None),
        P("sp", None, "tp"),
        P("sp", None, "tp"),
        P("sp", "tp", None),
    )
    return jax.shard_map(
        per_device, mesh=mesh, in_specs=placed, out_specs=P("sp", "tp"), check_vma=False
    )
```

profile of v0, /device:TPU:0, one launch (start us, length us, event | category | flops | bytes accessed | tf_op | source)
XLA Modules:
  0.0 212.3 jit_solution(1286813573739635724)
XLA Ops:
  7.4 4.9 %collective-permute-start.1 = (bf16[2]{0:T(256)(128)(2,1)S(1)}, bf16[2]{0:T(256)(128)(2,1)S(1)}, u32[]{:S(2)}, u32[]{:S(2)}) collective-permute-start(bf16[2]{0:T(256)(128)(2,1)S(1)} %slice.41), channel_id=1, source_target_pairs={{0,4},{4,8},{8,12},{12,16},{16,20},{20,24},{24,28},{1,5},{5,9},{9,... | collective-permute-start | bytes 20 | tf_op jit(solution)/shard_map/ppermute | solution.py:12
  12.2 0.9 multiply_convert_fusion.2
  13.1 3.5 %collective-permute-start = (bf16[2,128]{1,0:T(2,128)(2,1)S(1)}, bf16[2,128]{1,0:T(2,128)(2,1)S(1)}, u32[]{:S(2)}, u32[]{:S(2)}) collective-permute-start(bf16[2,128]{1,0:T(2,128)(2,1)S(1)} %slice.52), channel_id=1, source_target_pairs={{0,4},{4,8},{8,12},{12,16},{16,20},{20,24},{24,28},{1,5},{5,9},{9,... | collective-permute-start | bytes 1544 | tf_op jit(solution)/shard_map/ppermute | solution.py:12
  16.6 0.8 copy.17
  18.4 0.8 slice_bitcast_fusion.2
  19.2 1.1 reduce-window.6
  21.0 2.4 %scatter_custom_fusion = s32[1024]{0:T(1024)S(1)} fusion(s32[512]{0:T(512)S(1)} %bitcast.38, s32[512]{0:T(512)S(1)} %add_select_fusion, s32[]{:T(128)} %constant.38.clone.1), kind=kCustom, calls=%fused_computation.49 | custom fusion | bytes 4100 | tf_op jit(solution)/shard_map/scatter | solution.py:25
  23.6 0.8 compare_convert_fusion.1
  24.3 1.0 fusion.15
  25.3 5.8 %all_gather.6 = bf16[256,512]{1,0:T(8,128)(2,1)S(1)} all-gather(bf16[256,128]{1,0:T(8,128)(2,1)S(1)} %fusion.15), channel_id=1, replica_groups=mesh['sp'=8,'tp'=4] {'tp'}, dimensions={1}, use_global_device_ids=true | all-gather | bytes 327680 | tf_op jit(solution)/shard_map/all_gather | solution.py:63
  31.3 1.4 multiply_reduce_fusion.1
  32.7 7.1 %psum.7 = f32[256]{0:T(256)S(1)} all-reduce(f32[256]{0:T(256)S(1)} %get-tuple-element.10), channel_id=1, replica_groups=mesh['sp'=8,'tp'=4] {'tp'}, use_global_device_ids=true, to_apply=%region_2.0 | all-reduce | flops 256 | bytes 2048 | tf_op jit(solution)/shard_map/psum | solution.py:69
  39.9 4.0 %gather_fusion = bf16[1024,512]{1,0:T(8,128)(2,1)S(1)} fusion(bf16[257,512]{1,0:T(8,128)(2,1)S(1)} %concatenate.11, s32[1024]{0:T(1024)S(1)} %fusion.21), kind=kCustom, calls=%fused_computation | custom fusion | bytes 2101248 | tf_op jit(solution)/shard_map/gather | solution.py:78
  43.9 29.1 %all_to_all.10 = bf16[8,128,512]{2,1,0:T(8,128)(2,1)} all-to-all(bf16[8,128,512]{2,1,0:T(8,128)(2,1)S(1)} %bitcast.36), channel_id=1, replica_groups=mesh['sp'=8,'tp'=4] {'sp'}, dimensions={0} | all-to-all | bytes 2097152 | tf_op jit(solution)/shard_map/all_to_all | solution.py:79
  73.1 33.6 %all-gather.2.cloned.1.call-done = bf16[8,128,2048]{2,1,0:T(8,128)(2,1)} async-done(((bf16[8,128,512]{2,1,0:T(8,128)(2,1)}), bf16[8,128,2048]{2,1,0:T(8,128)(2,1)}) %all-gather.2.cloned.1.call-update) | async-done | bytes 4194320 | tf_op jit(solution)/shard_map/all_gather | solution.py:80
  106.6 7.5 %fusion.1 = f32[1024,896]{1,0:T(8,128)S(1)} fusion(bf16[1024,2048]{1,0:T(8,128)(2,1)} %bitcast.41, bf16[1,2048,896]{2,1,0:T(8,128)(2,1)} %param.26), kind=kOutput, calls=%fused_computation.5 | convolution fusion | flops 3758096384 | bytes 11534336 | tf_op jit(solution)/shard_map/dot_general | solution.py:83
  114.2 4.8 %multiply_convert_fusion = bf16[1024,896]{1,0:T(8,128)(2,1)S(1)} fusion(f32[1024,896]{1,0:T(8,128)S(1)} %fusion.1, bf16[1024,2048]{1,0:T(8,128)(2,1)S(1)} %bitcast.42, bf16[1,2048,896]{2,1,0:T(8,128)(2,1)S(1)} %copy-done.4), kind=kOutput, calls=%fused_computation.9 | convolution fusion | flops 3763601408 | bytes 13369344 | tf_op jit(solution)/shard_map/dot_general | solution.py:82
  118.9 6.1 %convolution_convert_fusion = bf16[1024,2048]{1,0:T(8,128)(2,1)} fusion(bf16[1024,896]{1,0:T(8,128)(2,1)S(1)} %multiply_convert_fusion, bf16[1,896,2048]{2,1,0:T(8,128)(2,1)S(1)} %copy-done.5), kind=kOutput, calls=%fused_computation.3 | convolution fusion | flops 3760193536 | bytes 9699328 | tf_op jit(solution)/shard_map/dot_general | solution.py:85
  125.0 44.6 %reduce-scatter.2.cloned.1.call-done = bf16[1024,512]{1,0:T(8,128)(2,1)} async-done(((bf16[1024,2048]{1,0:T(8,128)(2,1)}), bf16[1024,512]{1,0:T(8,128)(2,1)}) %reduce-scatter.2.cloned.1.call-update) | async-done | bytes 1048592 | tf_op jit(solution)/shard_map/reduce_scatter | solution.py:86
  169.6 5.5 %all-to-all-start.1 = ((bf16[8,128,512]{2,1,0:T(8,128)(2,1)}), bf16[8,128,512]{2,1,0:T(8,128)(2,1)S(1)}, u32[]{:S(2)}, u32[]{:S(2)}) async-start(bf16[8,128,512]{2,1,0:T(8,128)(2,1)} %bitcast.37), calls=%async_computation.2 | async-start | bytes 2097152 | tf_op jit(solution)/shard_map/all_to_all | solution.py:89
  175.2 25.5 %all-to-all-done.1 = bf16[8,128,512]{2,1,0:T(8,128)(2,1)S(1)} async-done(((bf16[8,128,512]{2,1,0:T(8,128)(2,1)}), bf16[8,128,512]{2,1,0:T(8,128)(2,1)S(1)}, u32[]{:S(2)}, u32[]{:S(2)}) %all-to-all-start.1) | async-done | bytes 1048608 | tf_op jit(solution)/shard_map/all_to_all | solution.py:89
  200.8 2.0 gather_fusion.1
  203.4 1.3 multiply_reduce_fusion
  204.7 0.8 add_convert_fusion
  (44 shorter events, 3.7 us)
Async XLA Ops:
  6.5 24.8 %copy-start = (bf16[512,512]{1,0:T(8,128)(2,1)S(1)}, bf16[512,512]{1,0:T(8,128)(2,1)}, u32[]{:S(2)}) copy-start(bf16[512,512]{1,0:T(8,128)(2,1)} %param.21) | copy-start | bytes 1572868
  6.5 33.2 %copy-start.1 = (f32[512]{0:T(512)S(1)}, f32[512]{0:T(512)}, u32[]{:S(2)}) copy-start(f32[512]{0:T(512)} %param.22) | copy-start | bytes 6148
  6.5 100.1 %all-gather.2.cloned.1.call-start = ((), (), s32[]{:S(2)}) async-start(), calls=%async_computation.3 | async-start | bytes 5242880 | tf_op jit(solution)/shard_map/all_gather | solution.py:80
  7.4 16.1 %collective-permute-start.1 = (bf16[2]{0:T(256)(128)(2,1)S(1)}, bf16[2]{0:T(256)(128)(2,1)S(1)}, u32[]{:S(2)}, u32[]{:S(2)}) collective-permute-start(bf16[2]{0:T(256)(128)(2,1)S(1)} %slice.41), channel_id=1, source_target_pairs={{0,4},{4,8},{8,12},{12,16},{16,20},{20,24},{24,28},{1,5},{5,9},{9,... | collective-permute-start | bytes 20 | tf_op jit(solution)/shard_map/ppermute | solution.py:12
  13.1 11.2 %collective-permute-start = (bf16[2,128]{1,0:T(2,128)(2,1)S(1)}, bf16[2,128]{1,0:T(2,128)(2,1)S(1)}, u32[]{:S(2)}, u32[]{:S(2)}) collective-permute-start(bf16[2,128]{1,0:T(2,128)(2,1)S(1)} %slice.52), channel_id=1, source_target_pairs={{0,4},{4,8},{8,12},{12,16},{16,20},{20,24},{24,28},{1,5},{5,9},{9,... | collective-permute-start | bytes 1544 | tf_op jit(solution)/shard_map/ppermute | solution.py:12
  73.0 96.6 %reduce-scatter.2.cloned.1.call-start = ((), (), s32[]{:S(2)}) async-start(), calls=%async_computation.4 | async-start | bytes 5242880 | tf_op jit(solution)/shard_map/reduce_scatter | solution.py:86
  106.6 7.5 %copy-start.3 = (bf16[8,128,2048]{2,1,0:T(8,128)(2,1)S(1)}, bf16[8,128,2048]{2,1,0:T(8,128)(2,1)}, u32[]{:S(2)}) copy-start(bf16[8,128,2048]{2,1,0:T(8,128)(2,1)} %all-gather.2.cloned.1.call-done) | copy-start | bytes 12582916
  106.6 7.5 %copy-start.4 = (bf16[1,2048,896]{2,1,0:T(8,128)(2,1)S(1)}, bf16[1,2048,896]{2,1,0:T(8,128)(2,1)}, u32[]{:S(2)}) copy-start(bf16[1,2048,896]{2,1,0:T(8,128)(2,1)} %param.25) | copy-start | bytes 11010052
  114.2 4.8 %copy-start.5 = (bf16[1,896,2048]{2,1,0:T(8,128)(2,1)S(1)}, bf16[1,896,2048]{2,1,0:T(8,128)(2,1)}, u32[]{:S(2)}) copy-start(bf16[1,896,2048]{2,1,0:T(8,128)(2,1)} %param.27) | copy-start | bytes 11010052
  125.0 50.1 %copy-start.2 = (f32[256,2]{0,1:T(2,128)S(1)}, f32[256,2]{0,1:T(2,128)}, u32[]{:S(2)}) copy-start(f32[256,2]{0,1:T(2,128)} %param.24) | copy-start | bytes 6148
  169.6 31.2 %all-to-all-start.1 = ((bf16[8,128,512]{2,1,0:T(8,128)(2,1)}), bf16[8,128,512]{2,1,0:T(8,128)(2,1)S(1)}, u32[]{:S(2)}, u32[]{:S(2)}) async-start(bf16[8,128,512]{2,1,0:T(8,128)(2,1)} %bitcast.37), calls=%async_computation.2 | async-start | bytes 2097152 | tf_op jit(solution)/shard_map/all_to_all | solution.py:89
Sparse Core Ops, SparseCore 0:
  73.1 33.4 all-gather.1
  125.1 44.3 reduce-scatter.1
where the time goes:
time: 213 us; the launch traced here: 212 us
  waiting for transfers between devices  104 us (49%)
  blocking collectives  42 us (20%)
  matrix products  19.7 us (9%)
  starting transfers between devices  13.9 us (7%)
  between operations  13.6 us (6%)
  local copies, waits for them, and re-layouts  11.7 us (5%)
  other arithmetic  7.8 us (4%)
    reduce_scatter x1, waiting for transfers between devices, per_device(): lax.psum_scatter(partial_out.astype(jnp.bfloat16), 'tp', scatter_dimensio...  44.6 us
    all_gather x1, waiting for transfers between devices, per_device(): arrived = lax.all_gather(slices_in, 'tp', axis=2, tiled=True)  33.6 us
    all_to_all x1, blocking collectives, per_device(): lax.all_to_all(outgoing, 'sp', split_axis=0, concat_axis=0, tiled=True)  29.1 us
    all_to_all x1, waiting for transfers between devices, per_device(): lax.all_to_all(summed.reshape(experts, capacity, local_features), 'sp', s...  25.5 us
    ppermute x2, starting transfers between devices, from_behind(): return lax.ppermute(block, axis, route)  8.32 us
    dot_general x1, matrix products, per_device(): upper = jnp.dot(expert_in, expert_up[0], preferred_element_type=jnp.float32)  7.49 us
    psum x1, blocking collectives, per_device(): feature_total = lax.psum(jnp.sum(hidden_state * hidden_state, axis=1), 'tp')  7.09 us
    dot_general x1, matrix products, per_device(): jnp.dot(act, expert_down[0], preferred_element_type=jnp.float32)  6.05 us
  transfers between devices with their start and end apart: 5, of which 3 were waited for; matrix products, arithmetic and copies ran while one was open for 4% of the time, Pallas kernels for 0%

commit v1 on v0

--- a/solution.py
+++ b/solution.py
@@ -77,7 +77,12 @@
     padded = jnp.concatenate([normed, jnp.zeros((1, local_features), jnp.bfloat16)], axis=0)
     outgoing = padded[owners].reshape(experts, capacity, local_features)
     slices_in = lax.all_to_all(outgoing, "sp", split_axis=0, concat_axis=0, tiled=True)
-    arrived = lax.all_gather(slices_in, "tp", axis=2, tiled=True)
+    ring = [slices_in]
+    for hop in range(3):
+        ring.append(lax.ppermute(ring[-1], "tp", [(dev, (dev + 1) % 4) for dev in range(4)]))
+    arrived = jnp.roll(
+        jnp.concatenate(ring[::-1], axis=2), (lax.axis_index("tp") + 1) * ring[0].shape[2], axis=2
+    )
     expert_in = arrived.reshape(-1, model_width)
     gate = jnp.dot(expert_in, expert_gate[0], preferred_element_type=jnp.float32)
     upper = jnp.dot(expert_in, expert_up[0], preferred_element_type=jnp.float32)

time: 213 us -> 227 us (1.066)
  local copies, waits for them, and re-layouts: 11.7 us -> 19.8 us
  waiting for transfers between devices: 104 us -> 112 us
  matrix products: 19.7 us -> 16.6 us
    ppermute x0 -> x3, waiting for transfers between devices: none -> 43.1 us  [per_device(): lax.ppermute(ring[-1], 'tp', [(dev, (dev + 1) % 4) for dev in range(4)])]
    all_gather x1 -> x0, waiting for transfers between devices: 33.6 us -> none  [per_device(): arrived = lax.all_gather(slices_in, 'tp', axis=2, tiled=True)]
    unnamed x14 -> x19, local copies, waits for them, and re-layouts: 0.97 us -> 8.65 us
    dot_general x1, matrix products: 7.49 us -> 4.69 us  [per_device(): upper = jnp.dot(expert_in, expert_up[0], preferred_element_type=jnp.float32)]
  transfers between devices with their start and end apart: 5 -> 7, of which waited for: 3 -> 5; matrix products, arithmetic and copies ran while one was open for 4% -> 4% of each run, Pallas kernels for 0% -> 0%
where the time goes in v1:
time: 227 us
  waiting for transfers between devices  112 us (49%)
  blocking collectives  41.9 us (18%)
  local copies, waits for them, and re-layouts  19.8 us (9%)
  matrix products  16.6 us (7%)
  starting transfers between devices  13.8 us (6%)
  between operations  13.7 us (6%)
  other arithmetic  8.49 us (4%)
    reduce_scatter x1, waiting for transfers between devices, per_device(): lax.psum_scatter(partial_out.astype(jnp.bfloat16), 'tp', scatter_dimensio...  43.6 us
    ppermute x3, waiting for transfers between devices, per_device(): lax.ppermute(ring[-1], 'tp', [(dev, (dev + 1) % 4) for dev in range(4)])  43.1 us
    all_to_all x1, blocking collectives, per_device(): lax.all_to_all(outgoing, 'sp', split_axis=0, concat_axis=0, tiled=True)  29 us
    all_to_all x1, waiting for transfers between devices, per_device(): lax.all_to_all(summed.reshape(experts, capacity, local_features), 'sp', s...  25.5 us
    unnamed x19, local copies, waits for them, and re-layouts  8.65 us
    ppermute x2, starting transfers between devices, from_behind(): return lax.ppermute(block, axis, route)  8.32 us
    psum x1, blocking collectives, per_device(): feature_total = lax.psum(jnp.sum(hidden_state * hidden_state, axis=1), 'tp')  7.1 us
    dot_general x1, matrix products, per_device(): jnp.dot(act, expert_down[0], preferred_element_type=jnp.float32)  6.08 us
  transfers between devices with their start and end apart: 7, of which 5 were waited for; matrix products, arithmetic and copies ran while one was open for 4% of the time, Pallas kernels for 0%

profile of v1, /device:TPU:0, one launch (start us, length us, event | category | flops | bytes accessed | tf_op | source)
XLA Modules:
  0.0 226.5 jit_solution(12594228489039411789)
XLA Ops:
  7.4 4.9 %collective-permute-start.1 = (bf16[2]{0:T(256)(128)(2,1)S(1)}, bf16[2]{0:T(256)(128)(2,1)S(1)}, u32[]{:S(2)}, u32[]{:S(2)}) collective-permute-start(bf16[2]{0:T(256)(128)(2,1)S(1)} %slice.41), channel_id=1, source_target_pairs={{0,4},{4,8},{8,12},{12,16},{16,20},{20,24},{24,28},{1,5},{5,9},{9,... | collective-permute-start | bytes 20 | tf_op jit(solution)/shard_map/ppermute | solution.py:12
  13.1 3.5 %collective-permute-start = (bf16[2,128]{1,0:T(2,128)(2,1)S(1)}, bf16[2,128]{1,0:T(2,128)(2,1)S(1)}, u32[]{:S(2)}, u32[]{:S(2)}) collective-permute-start(bf16[2,128]{1,0:T(2,128)(2,1)S(1)} %slice.52), channel_id=1, source_target_pairs={{0,4},{4,8},{8,12},{12,16},{16,20},{20,24},{24,28},{1,5},{5,9},{9,... | collective-permute-start | bytes 1544 | tf_op jit(solution)/shard_map/ppermute | solution.py:12
  21.0 2.4 %scatter_custom_fusion = s32[1024]{0:T(1024)S(1)} fusion(s32[512]{0:T(512)S(1)} %bitcast.40, s32[512]{0:T(512)S(1)} %add_select_fusion, s32[]{:T(128)} %constant.61.clone.1), kind=kCustom, calls=%fused_computation.57 | custom fusion | bytes 4100 | tf_op jit(solution)/shard_map/scatter | solution.py:25
  25.3 5.8 %all_gather.3 = bf16[256,512]{1,0:T(8,128)(2,1)S(1)} all-gather(bf16[256,128]{1,0:T(8,128)(2,1)S(1)} %fusion.15), channel_id=1, replica_groups=mesh['sp'=8,'tp'=4] {'tp'}, dimensions={1}, use_global_device_ids=true | all-gather | bytes 327680 | tf_op jit(solution)/shard_map/all_gather | solution.py:63
  31.3 1.4 multiply_reduce_fusion.1
  32.7 7.1 %psum.7 = f32[256]{0:T(256)S(1)} all-reduce(f32[256]{0:T(256)S(1)} %get-tuple-element.10), channel_id=1, replica_groups=mesh['sp'=8,'tp'=4] {'tp'}, use_global_device_ids=true, to_apply=%region_2.0 | all-reduce | flops 256 | bytes 2048 | tf_op jit(solution)/shard_map/psum | solution.py:69
  40.6 4.0 %gather_fusion = bf16[1024,512]{1,0:T(8,128)(2,1)S(1)} fusion(bf16[257,512]{1,0:T(8,128)(2,1)S(1)} %concatenate.17, s32[1024]{0:T(1024)S(1)} %fusion.21), kind=kCustom, calls=%fused_computation | custom fusion | bytes 2101248 | tf_op jit(solution)/shard_map/gather | solution.py:78
  44.6 29.0 %all_to_all.10 = bf16[8,128,512]{2,1,0:T(8,128)(2,1)S(1)} all-to-all(bf16[8,128,512]{2,1,0:T(8,128)(2,1)S(1)} %bitcast.36), channel_id=1, replica_groups=mesh['sp'=8,'tp'=4] {'sp'}, dimensions={0} | all-to-all | bytes 2097152 | tf_op jit(solution)/shard_map/all_to_all | solution.py:79
  73.5 14.2 %collective-permute-done.2 = bf16[8,128,512]{2,1,0:T(8,128)(2,1)S(1)} collective-permute-done((bf16[8,128,512]{2,1,0:T(8,128)(2,1)S(1)}, bf16[8,128,512]{2,1,0:T(8,128)(2,1)S(1)}, u32[]{:S(2)}, u32[]{:S(2)}) %collective-permute-start.2) | collective-permute-done | bytes 1048608 | tf_op jit(solution)/shard_map/ppermute | solution.py:82
  87.8 14.3 %collective-permute-done.3 = bf16[8,128,512]{2,1,0:T(8,128)(2,1)} collective-permute-done((bf16[8,128,512]{2,1,0:T(8,128)(2,1)S(1)}, bf16[8,128,512]{2,1,0:T(8,128)(2,1)}, u32[]{:S(2)}, u32[]{:S(2)}) %collective-permute-start.3) | collective-permute-done | bytes 1048608 | tf_op jit(solution)/shard_map/ppermute | solution.py:82
  102.1 14.5 %collective-permute-done.4 = bf16[8,128,512]{2,1,0:T(8,128)(2,1)} collective-permute-done((bf16[8,128,512]{2,1,0:T(8,128)(2,1)}, bf16[8,128,512]{2,1,0:T(8,128)(2,1)}, u32[]{:S(2)}, u32[]{:S(2)}) %collective-permute-start.4) | collective-permute-done | bytes 1048608 | tf_op jit(solution)/shard_map/ppermute | solution.py:82
  116.6 1.4 constant_dynamic-update-slice_fusion.7
  118.0 1.4 constant_dynamic-update-slice_fusion.6
  119.7 1.4 constant_dynamic-update-slice_fusion.3
  121.1 1.4 constant_dynamic-update-slice_fusion.2
  123.2 1.7 copy-done.2
  124.9 4.5 %fusion.3 = f32[1024,896]{1,0:T(8,128)S(1)} fusion(bf16[1024,2048]{1,0:T(8,128)(2,1)S(1)} %bitcast.37, bf16[1,2048,896]{2,1,0:T(8,128)(2,1)S(1)} %copy-done.2), kind=kOutput, calls=%fused_computation.7 | convolution fusion | flops 3758096384 | bytes 11534336 | tf_op jit(solution)/shard_map/dot_general | solution.py:87
  129.4 4.7 %multiply_convert_fusion = bf16[1024,896]{1,0:T(8,128)(2,1)S(1)} fusion(f32[1024,896]{1,0:T(8,128)S(1)} %fusion.3, bf16[1024,2048]{1,0:T(8,128)(2,1)S(1)} %bitcast.38, bf16[1,2048,896]{2,1,0:T(8,128)(2,1)S(1)} %copy-done.3), kind=kOutput, calls=%fused_computation.9 | convolution fusion | flops 3763601408 | bytes 13369344 | tf_op jit(solution)/shard_map/dot_general | solution.py:88
  134.1 6.1 %convolution_convert_fusion = bf16[1024,2048]{1,0:T(8,128)(2,1)} fusion(bf16[1024,896]{1,0:T(8,128)(2,1)S(1)} %multiply_convert_fusion, bf16[1,896,2048]{2,1,0:T(8,128)(2,1)S(1)} %copy-done.4), kind=kOutput, calls=%fused_computation.3 | convolution fusion | flops 3760193536 | bytes 9699328 | tf_op jit(solution)/shard_map/dot_general | solution.py:90
  140.2 43.6 %reduce-scatter.2.cloned.1.call-done = bf16[1024,512]{1,0:T(8,128)(2,1)} async-done(((bf16[1024,2048]{1,0:T(8,128)(2,1)}), bf16[1024,512]{1,0:T(8,128)(2,1)}) %reduce-scatter.2.cloned.1.call-update) | async-done | bytes 1048592 | tf_op jit(solution)/shard_map/reduce_scatter | solution.py:91
  183.8 5.5 %all-to-all-start.1 = ((bf16[8,128,512]{2,1,0:T(8,128)(2,1)}), bf16[8,128,512]{2,1,0:T(8,128)(2,1)S(1)}, u32[]{:S(2)}, u32[]{:S(2)}) async-start(bf16[8,128,512]{2,1,0:T(8,128)(2,1)} %bitcast.39), calls=%async_computation.2 | async-start | bytes 2097152 | tf_op jit(solution)/shard_map/all_to_all | solution.py:94
  189.5 25.5 %all-to-all-done.1 = bf16[8,128,512]{2,1,0:T(8,128)(2,1)S(1)} async-done(((bf16[8,128,512]{2,1,0:T(8,128)(2,1)}), bf16[8,128,512]{2,1,0:T(8,128)(2,1)S(1)}, u32[]{:S(2)}, u32[]{:S(2)}) %all-to-all-start.1) | async-done | bytes 1048608 | tf_op jit(solution)/shard_map/all_to_all | solution.py:94
  215.0 2.0 gather_fusion.1
  217.6 1.3 multiply_reduce_fusion
  (54 shorter events, 11.4 us)
Async XLA Ops:
  6.5 24.8 %copy-start = (bf16[512,512]{1,0:T(8,128)(2,1)S(1)}, bf16[512,512]{1,0:T(8,128)(2,1)}, u32[]{:S(2)}) copy-start(bf16[512,512]{1,0:T(8,128)(2,1)} %param.21) | copy-start | bytes 1572868
  6.5 177.2 %reduce-scatter.2.cloned.1.call-start = ((), (), s32[]{:S(2)}) async-start(), calls=%async_computation.3 | async-start | bytes 5242880 | tf_op jit(solution)/shard_map/reduce_scatter | solution.py:91
  7.4 16.1 %collective-permute-start.1 = (bf16[2]{0:T(256)(128)(2,1)S(1)}, bf16[2]{0:T(256)(128)(2,1)S(1)}, u32[]{:S(2)}, u32[]{:S(2)}) collective-permute-start(bf16[2]{0:T(256)(128)(2,1)S(1)} %slice.41), channel_id=1, source_target_pairs={{0,4},{4,8},{8,12},{12,16},{16,20},{20,24},{24,28},{1,5},{5,9},{9,... | collective-permute-start | bytes 20 | tf_op jit(solution)/shard_map/ppermute | solution.py:12
  13.1 11.2 %collective-permute-start = (bf16[2,128]{1,0:T(2,128)(2,1)S(1)}, bf16[2,128]{1,0:T(2,128)(2,1)S(1)}, u32[]{:S(2)}, u32[]{:S(2)}) collective-permute-start(bf16[2,128]{1,0:T(2,128)(2,1)S(1)} %slice.52), channel_id=1, source_target_pairs={{0,4},{4,8},{8,12},{12,16},{16,20},{20,24},{24,28},{1,5},{5,9},{9,... | collective-permute-start | bytes 1544 | tf_op jit(solution)/shard_map/ppermute | solution.py:12
  73.5 14.2 %collective-permute-start.2 = (bf16[8,128,512]{2,1,0:T(8,128)(2,1)S(1)}, bf16[8,128,512]{2,1,0:T(8,128)(2,1)S(1)}, u32[]{:S(2)}, u32[]{:S(2)}) collective-permute-start(bf16[8,128,512]{2,1,0:T(8,128)(2,1)S(1)} %all_to_all.10), channel_id=1, source_target_pairs={{0,1},{1,2},{2,3},{3,0},{4,5},{5,6},{6,7},{7,4},{8,9},{9,10},{10,1... | collective-permute-start | bytes 3145736 | tf_op jit(solution)/shard_map/ppermute | solution.py:82
  87.8 14.3 %collective-permute-start.3 = (bf16[8,128,512]{2,1,0:T(8,128)(2,1)S(1)}, bf16[8,128,512]{2,1,0:T(8,128)(2,1)}, u32[]{:S(2)}, u32[]{:S(2)}) collective-permute-start(bf16[8,128,512]{2,1,0:T(8,128)(2,1)S(1)} %collective-permute-done.2), channel_id=1, source_target_pairs={{0,1},{1,2},{2,3},{3,0},{4,5},{5,6},{6,7},{7,4},{8,9},{9,10},{10,1... | collective-permute-start | bytes 3145736 | tf_op jit(solution)/shard_map/ppermute | solution.py:82
  102.1 14.5 %collective-permute-start.4 = (bf16[8,128,512]{2,1,0:T(8,128)(2,1)}, bf16[8,128,512]{2,1,0:T(8,128)(2,1)}, u32[]{:S(2)}, u32[]{:S(2)}) collective-permute-start(bf16[8,128,512]{2,1,0:T(8,128)(2,1)} %collective-permute-done.3), channel_id=1, source_target_pairs={{0,1},{1,2},{2,3},{3,0},{4,5},{5,6},{6,7},{7,4},{8,9},{9,10},{10,1... | collective-permute-start | bytes 3145736 | tf_op jit(solution)/shard_map/ppermute | solution.py:82
  122.8 2.0 copy-start.2
  124.9 4.5 %copy-start.3 = (bf16[1,2048,896]{2,1,0:T(8,128)(2,1)S(1)}, bf16[1,2048,896]{2,1,0:T(8,128)(2,1)}, u32[]{:S(2)}) copy-start(bf16[1,2048,896]{2,1,0:T(8,128)(2,1)} %param.26) | copy-start | bytes 11010052
  129.4 4.7 %copy-start.4 = (bf16[1,896,2048]{2,1,0:T(8,128)(2,1)S(1)}, bf16[1,896,2048]{2,1,0:T(8,128)(2,1)}, u32[]{:S(2)}) copy-start(bf16[1,896,2048]{2,1,0:T(8,128)(2,1)} %param.27) | copy-start | bytes 11010052
  140.2 49.1 %copy-start.1 = (f32[256,2]{0,1:T(2,128)S(1)}, f32[256,2]{0,1:T(2,128)}, u32[]{:S(2)}) copy-start(f32[256,2]{0,1:T(2,128)} %param.24) | copy-start | bytes 6148
  183.8 31.2 %all-to-all-start.1 = ((bf16[8,128,512]{2,1,0:T(8,128)(2,1)}), bf16[8,128,512]{2,1,0:T(8,128)(2,1)S(1)}, u32[]{:S(2)}, u32[]{:S(2)}) async-start(bf16[8,128,512]{2,1,0:T(8,128)(2,1)} %bitcast.39), calls=%async_computation.2 | async-start | bytes 2097152 | tf_op jit(solution)/shard_map/all_to_all | solution.py:94
Sparse Core Ops, SparseCore 0:
  140.3 43.4 reduce-scatter.1
